TPU v7x, 32 devices: a whole 2x2x4 slice. The times are simulated.
32 devices in a mesh: sp: 8 (over z, y), tp: 4 (over x, core).
Axes of the slice: x: 2, y: 2, z: 4, core: 2. Of those that a mesh axis runs over, the one named last changes fastest.
Arguments:
- queries: bfloat16 [8192, 1024], P('sp', 'tp'), may hold values from -6 to 6
- keys: bfloat16 [8192, 1024], P('sp', 'tp'), may hold values from -6 to 6
- values: bfloat16 [8192, 2048], P('sp', 'tp'), may hold values from -6 to 6
- output_gate_logits: bfloat16 [8192, 2048], P('sp', 'tp'), may hold values from -6 to 6
- log_input_gate: float32 [16, 8192], P('tp', 'sp'), may hold values from -4 to 104, as said below
- forget_gate_logits: float32 [16, 8192], P('tp', 'sp'), may hold values from 1 to 20
- extra_forget_terms: float32 [16, 8192], P('tp', 'sp'), may hold values from -2.1 to 0, as said below
- per_head_norm_gain: float32 [2048], P('tp'), may hold values from 0.1 to 1.9
- output_weight: bfloat16 [2048, 2048], P('tp'), may hold values from -0.125 to 0.125
- residual: bfloat16 [8192, 2048], P(('sp', 'tp')), may hold values from -6 to 6
- after_cell_norm_gain: float32 [2048], replicated, may hold values from 0.1 to 1.9
- feedforward_norm_gain: float32 [2048], replicated, may hold values from 0.1 to 1.9
- closing_norm_gain: float32 [2048], replicated, may hold values from 0.1 to 1.9
- gate_up_weight: bfloat16 [2048, 5632], P('sp', 'tp'), may hold values from -0.125 to 0.125
- value_up_weight: bfloat16 [2048, 5632], P('sp', 'tp'), may hold values from -0.125 to 0.125
- gate_filter_taps: bfloat16 [3, 5632], P(None, 'tp'), may hold values from -3 to 3
- value_filter_taps: bfloat16 [3, 5632], P(None, 'tp'), may hold values from -3 to 3
- down_weight: bfloat16 [5632, 2048], P('tp', 'sp'), may hold values from -0.078125 to 0.078125
Outputs:
- result: bfloat16 [8192, 2048], P(('sp', 'tp'))
Inputs may be any that keep to these rules, and one draw needn't show every extreme that they name: log_input_gate is a log gate of order one at most positions and may be far larger at a few. extra_forget_terms is zero at nearly all positions.
All inputs are finite; a program needn't handle non-finite values.
Results may differ from a plain program's by a relative error of at most 0.019.
Values may be sent and summed in bfloat16 or wider, within the bound.
A program may use at most 128 MiB of HBM per device.

v0:
```python
import functools

import jax
import jax.numpy as jnp
from jax import lax
from jax.experimental import pallas as pl
from jax.experimental.pallas import tpu as pltpu
from jax.sharding import PartitionSpec as P

MESH = pl.DeviceIdType.MESH
CORES = 2
KEY_DIM = 64
VAL_DIM = 128
WIDTH = 3
LANES = 128
CHUNK = 128
HALO = 16
VMEM_BYTES = 67_000_000

eps = 1e-06
empty_log = -1e30
f32, bf16 = jnp.float32, jnp.bfloat16


def rms_scale(total_square, width):
    return lax.rsqrt(total_square / width + eps)


def rms_gain(inputs, gains):
    return inputs * lax.rsqrt(jnp.mean(inputs * inputs, axis=-1, keepdims=True) + eps) * gains


def remote(src, dst, send, recv, where):
    return pltpu.make_async_remote_copy(
        src_ref=src,
        dst_ref=dst,
        send_sem=send,
        recv_sem=recv,
        device_id=where,
        device_id_type=MESH,
    )


def mm(left, right):
    return jnp.dot(left, right, preferred_element_type=f32)


def split(array):
    high = array.astype(bf16)
    return high, (array - high.astype(f32)).astype(bf16)


def scan_lanes(array, op, neutral):
    length = array.shape[1]
    lane = lax.broadcasted_iota(jnp.int32, array.shape, 1)
    shift = 1
    while shift < length:
        moved = pltpu.roll(array, shift, 1)
        array = op(array, jnp.where(lane >= shift, moved, neutral))
        shift *= 2
    return array


def grid_of(count):
    rows_y = 1
    while 8 * rows_y * rows_y <= count:
        rows_y *= 2
    return count // rows_y, rows_y


def to_sp(place, count):
    rows_z, rows_y = grid_of(count)
    at_y, k = place // rows_z, lax.rem(place, rows_z)
    at_z = jnp.where(lax.rem(at_y, 2) == 0, k, rows_z - 1 - k)
    return at_z * rows_y + at_y


def to_place(sp, count):
    rows_z, rows_y = grid_of(count)
    at_z, at_y = sp // rows_y, lax.rem(sp, rows_y)
    return at_y * rows_z + jnp.where(lax.rem(at_y, 2) == 0, at_z, rows_z - 1 - at_z)


def reach_of(count, way, half):
    return count // 2 if way == half else count // 2 - 1


def ring_events(count):
    ways = []
    for way in range(2):
        events = []
        for kind in ("up", "down"):
            for hop in range(1, count // 2 + 1):
                for half in range(2):
                    if hop <= reach_of(count, way, half):
                        for part in range(2 if kind == "up" else 1):
                            events.append((kind, half, part, hop))
        ways.append(events)
    return ways


class Ring:
    def __init__(self, count, up_own, up_all, down_own, down_all, send, recv):
        self.count = count
        self.up_own, self.up_all = up_own, up_all
        self.down_own, self.down_all = down_own, down_all
        self.send, self.recv = send, recv
        self.place = to_place(lax.axis_index("sp"), count)
        self.events = ring_events(count)
        self.at = [{e: i for i, e in enumerate(events)} for events in self.events]
        self.waited = set()
        self.sent = []
        self.next = 0

    def piece(self, kind, half, part, shard, own):
        if kind == "up":
            tiles, rows = self.up_own.shape[0], self.up_own.shape[1]
            low = (tiles + 1) // 2
            span = pl.ds(0, low) if part == 0 else pl.ds(low, tiles - low)
            if tiles == 1:
                return None if part else self._up(pl.ds(0, 1), half, shard, rows, own)
            return self._up(span, half, shard, rows, own)
        rows = self.down_own.shape[0] // 2
        span = pl.ds(half * rows, rows)
        return self.down_own.at[span] if own else self.down_all.at[shard, span]

    def _up(self, span, half, shard, rows, own):
        if own:
            return self.up_own.at[span, pl.ds(half * (rows // 2), rows // 2)]
        start = pl.multiple_of(shard * rows + half * (rows // 2), rows // 2)
        return self.up_all.at[span, pl.ds(start, rows // 2)]

    def shard(self, way, hop):
        step = hop if way == 0 else self.count - hop
        return to_sp(lax.rem(self.place + self.count - step, self.count), self.count)

    def copy(self, way, event, target):
        kind, half, part, hop = event
        at = self.at[way][event]
        shard = self.shard(way, hop - 1)
        src = self.piece(kind, half, part, shard, hop == 1)
        dst = self.piece(kind, half, part, shard, False)
        return remote(src, dst, self.send.at[way, at], self.recv.at[way, at], target)

    def arrived(self, way, event):
        if (way, event) in self.waited:
            return
        self.waited.add((way, event))
        kind, half, part, hop = event
        at = self.at[way][event]
        came = self.piece(kind, half, part, self.shard(way, hop), False)
        where = {"sp": self.shard(way, 1)}
        remote(came, came, self.send.at[way, at], self.recv.at[way, at], where).wait_recv()

    def pump(self, times=1):
        for _ in range(times):
            if self.next >= len(self.events[0]):
                return
            for way in range(2):
                event = self.events[way][self.next]
                kind, half, part, hop = event
                if hop > 1:
                    self.arrived(way, (kind, half, part, hop - 1))
                target = {"sp": self.shard(1 - way, 1)}
                copy = self.copy(way, event, target)
                copy.start()
                self.sent.append(copy)
            self.next += 1

    def pump_to(self, number):
        self.pump(max(number - self.next, 0))

    def arrived_all(self, kind, hop=None):
        for way in range(2):
            for event in self.events[way]:
                if event[0] == kind and (hop is None or event[3] == hop):
                    self.arrived(way, event)


def tp_places(count):
    me = lax.axis_index("tp")
    at_x, core = me // CORES, lax.rem(me, CORES)
    xs = count // CORES
    partner = at_x * CORES + 1 - core
    peers = [lax.rem(at_x + k, xs) * CORES + core for k in range(xs)]
    sources = [lax.rem(at_x + xs - k, xs) * CORES + core for k in range(xs)]
    return me, at_x, core, partner, peers, sources


def columns_of(rows):
    depth = rows.shape[0]
    if depth < LANES:
        rows = jnp.concatenate([rows, jnp.zeros((LANES - depth, LANES), f32)], axis=0)
    return rows.T


def column(turned, at):
    return jnp.broadcast_to(turned[:, at : at + 1], (turned.shape[0], LANES))


def wide(array):
    return jnp.concatenate([array, array], axis=1)


def gate_rows_into(heads, gate_ref, forget_ref, extra_ref, reach_ref, top_ref, cum_ref):
    def full(ref):
        array = ref[...]
        return jnp.concatenate([array] * (8 // heads), axis=0)

    logits = full(forget_ref)
    cum = scan_lanes(full(extra_ref) - jnp.log1p(jnp.exp(-logits)), jnp.add, 0.0)
    reach = full(gate_ref) - cum
    cum_ref[...] = cum
    reach_ref[...] = reach
    top_ref[...] = scan_lanes(reach, jnp.maximum, empty_log)


def cell_block(heads, b, q_ref, k_ref, v_ref, reach_ref, top_ref, num_ref, den_ref, state_ref, held_ref):
    rows = pl.ds(pl.multiple_of(b * CHUNK, CHUNK), CHUNK)
    reach, top = reach_ref[:, rows], top_ref[:, rows]
    before = held_ref[...]
    now = jnp.broadcast_to(jnp.max(top, axis=1, keepdims=True), top.shape)
    held_ref[...] = now
    turned = columns_of(jnp.concatenate([top, jnp.exp(before - top)], axis=0))
    fade = jnp.exp(before - now)
    weight = jnp.exp(reach - now)
    at_t = lax.broadcasted_iota(jnp.int32, (CHUNK, CHUNK), 0)
    at_s = lax.broadcasted_iota(jnp.int32, (CHUNK, CHUNK), 1)
    causal = at_s <= at_t
    ones = jnp.ones((CHUNK, LANES), bf16)
    for pair in range(heads // 2):
        pair_cols = pl.ds(pair * LANES, LANES)
        query = q_ref[rows, pair_cols]
        turned_keys = k_ref[rows, pair_cols].astype(f32).T
        for h in (2 * pair, 2 * pair + 1):
            cols = pl.ds(h * VAL_DIM, VAL_DIM)
            value = jnp.concatenate([v_ref[rows, cols], ones], axis=1)
            own = (at_t >= KEY_DIM) if h % 2 else (at_t < KEY_DIM)
            keys = jnp.where(own, turned_keys, 0.0)
            decay = jnp.exp(jnp.where(causal, reach[h : h + 1, :] - column(turned, h), empty_log))
            high, low = split(mm(query, keys.astype(bf16)) * decay)
            state = state_ref[h]
            state_high, state_low = split(state)
            carried = mm(query, state_high) + mm(query, state_low)
            total = mm(high, value) + mm(low, value) + wide(column(turned, 8 + h)) * carried
            num_ref[rows, cols] = total[:, :LANES]
            den_ref[rows, cols] = total[:, LANES:]
            high, low = split(keys * weight[h : h + 1, :])
            state_ref[h] = state * wide(fade[h : h + 1, :]) + mm(high, value) + mm(low, value)


def pack_state(heads, state_ref, held_ref, cum_last, cells_ref, small_ref):
    pairs = heads // 2
    rows = []
    for pair in range(pairs):
        both = state_ref[2 * pair] + state_ref[2 * pair + 1]
        cells_ref[pair] = both[:, :LANES]
        rows.append(both[:, LANES:].T[0:1, :])
    tops = held_ref[0:heads, :] + cum_last[0:heads, :]
    rows += [tops, cum_last[0:heads, :]]
    used = pairs + 2 * heads
    rows.append(jnp.zeros((small_ref.shape[0] - used, LANES), f32))
    small_ref[...] = jnp.concatenate(rows, axis=0)


def merge_state(heads, cells_ref, small_ref, in_cells, in_norm, in_top, in_after):
    pairs = heads // 2
    small = small_ref[...]
    tops, totals = small[pairs : pairs + heads, :], small[pairs + heads : pairs + 2 * heads, :]
    top, after = in_top[0:heads, :], in_after[0:heads, :]
    reach = after + tops
    best = jnp.maximum(top, reach)
    old, new = jnp.exp(top - best), jnp.exp(reach - best)
    in_top[0:heads, :] = best
    in_after[0:heads, :] = after + totals
    lane = lax.broadcasted_iota(jnp.int32, (1, LANES), 1) < KEY_DIM
    row = lax.broadcasted_iota(jnp.int32, (LANES, LANES), 0) < KEY_DIM
    for pair in range(pairs):
        a, b = slice(2 * pair, 2 * pair + 1), slice(2 * pair + 1, 2 * pair + 2)
        in_norm[pair : pair + 1, :] = (
            jnp.where(lane, old[a], old[b]) * in_norm[pair : pair + 1, :]
            + jnp.where(lane, new[a], new[b]) * small[pair : pair + 1, :]
        )
        in_cells[pair] = (
            jnp.where(row, old[a], old[b]) * in_cells[pair]
            + jnp.where(row, new[a], new[b]) * cells_ref[pair]
        )


def mix_block(
    heads, b, q_ref, gate_ref, gain_ref, top_ref, cum_ref, num_ref, den_ref, in_top, enter_ref, mixed_ref
):
    rows = pl.ds(pl.multiple_of(b * CHUNK, CHUNK), CHUNK)
    top, cum, came = top_ref[:, rows], cum_ref[:, rows], in_top[...]
    best = jnp.maximum(top, came)
    turned = columns_of(
        jnp.concatenate([jnp.exp(top - best), jnp.exp(came - best), jnp.exp(-(cum + best))], axis=0)
    )
    scale = KEY_DIM ** (-0.5)
    for pair in range(heads // 2):
        query = q_ref[rows, pl.ds(pair * LANES, LANES)]
        for h in (2 * pair, 2 * pair + 1):
            cols = pl.ds(h * VAL_DIM, VAL_DIM)
            carried = mm(query, enter_ref[0, h]) + mm(query, enter_ref[1, h])
            here, there, floor = column(turned, h), column(turned, 8 + h), column(turned, 16 + h)
            num = (here * num_ref[rows, cols] + there * carried[:, :LANES]) * scale
            den = (here * den_ref[rows, cols] + there * carried[:, LANES:]) * scale
            out = num / jnp.maximum(jnp.abs(den), floor)
            gate = jax.nn.sigmoid(gate_ref[rows, cols].astype(f32))
            mixed_ref[rows, cols] = (out * gain_ref[:, cols] * gate).astype(bf16)


def step_kernel(
    count, sps, pieces,
    q_ref, k_ref, v_ref, out_gate_ref, in_gate_ref, forget_ref, extra_ref, head_gain_ref,
    out_weight_ref, residual_ref, cell_gain_ref, ffn_gain_ref, close_gain_ref,
    up_own, gate_taps_ref, value_taps_ref, down_own,
    out_ref,
    up_all, down_all,
    reach_ref, top_ref, cum_ref, num_ref, den_ref, state_ref, held_ref,
    cells_out, small_out, cells_in, small_in, in_cells, in_norm, in_top, in_after, enter_ref,
    mixed_ref, total, pair_out, pair_in, x_out, x_in, after_ref, normed_ref, lift_ref, active_ref,
    total2, pair_out2, pair_in2, x_out2, x_in2,
    ring_send, ring_recv, own_sems, s_send, s_recv, t_send, t_recv, h_sems,
    pair_send, pair_recv, x_send, x_recv, gx_send, gx_recv, gp_send, gp_recv,
    p2_send, p2_recv, x2_send, x2_recv,
):
    sp = lax.axis_index("sp")
    me, at_x, core, partner, peers, sources = tp_places(count)
    xs = count // CORES
    tok_rows, heads = q_ref.shape[0], in_gate_ref.shape[0]
    blocks = tok_rows // CHUNK
    rows = tok_rows // count
    step = rows // pieces
    width = out_weight_ref.shape[1]
    ring = Ring(sps, up_own, up_all, down_own, down_all, ring_send, ring_recv)

    barrier = pltpu.get_barrier_semaphore()
    for d in range(1, sps):
        pl.semaphore_signal(
            barrier, inc=1, device_id={"sp": lax.rem(sp + d, sps)}, device_id_type=MESH
        )
    for where in [partner] + peers[1:]:
        pl.semaphore_signal(barrier, inc=1, device_id={"tp": where}, device_id_type=MESH)
    pl.semaphore_wait(barrier, sps - 1 + xs)

    ring.pump_to(PUMP_START)
    own_rows = up_own.shape[1]
    own_up = pltpu.make_async_copy(
        up_own,
        up_all.at[:, pl.ds(pl.multiple_of(sp * own_rows, own_rows), own_rows)],
        own_sems.at[0],
    )
    own_up.start()
    own_down = pltpu.make_async_copy(down_own, down_all.at[sp], own_sems.at[1])
    own_down.start()

    gate_rows_into(heads, in_gate_ref, forget_ref, extra_ref, reach_ref, top_ref, cum_ref)
    state_ref[...] = jnp.zeros_like(state_ref)
    held_ref[...] = jnp.full_like(held_ref, empty_log)

    @pl.loop(0, blocks)
    def _(b):
        cell_block(
            heads, b, q_ref, k_ref, v_ref, reach_ref, top_ref, num_ref, den_ref, state_ref, held_ref
        )

    last = cum_ref[:, pl.ds(tok_rows - LANES, LANES)]
    cum_last = jnp.broadcast_to(last[:, LANES - 1 :], last.shape)
    pack_state(heads, state_ref, held_ref, cum_last, cells_out, small_out)
    for d in range(1, sps):
        ahead = {"sp": lax.rem(sp + d, sps)}

        @pl.when(sp + d < sps)
        def _(d=d, ahead=ahead):
            remote(small_out, small_in.at[d], t_send.at[d], t_recv.at[d], ahead).start()
            remote(cells_out, cells_in.at[d], s_send.at[d], s_recv.at[d], ahead).start()

    ring.pump_to(PUMP_STATE)
    in_cells[...] = jnp.zeros_like(in_cells)
    in_norm[...] = jnp.zeros_like(in_norm)
    in_top[...] = jnp.full_like(in_top, empty_log)
    in_after[...] = jnp.zeros_like(in_after)
    for d in range(1, sps):

        @pl.when(sp - d >= 0)
        def _(d=d):
            behind = {"sp": lax.rem(sp + sps - d, sps)}
            remote(small_out, small_in.at[d], t_send.at[d], t_recv.at[d], behind).wait_recv()
            remote(cells_out, cells_in.at[d], s_send.at[d], s_recv.at[d], behind).wait_recv()
            merge_state(
                heads, cells_in.at[d], small_in.at[d], in_cells, in_norm, in_top, in_after
            )

    for pair in range(heads // 2):
        norm = jnp.broadcast_to(in_norm[pair : pair + 1, :], (LANES, LANES)).T
        full = jnp.concatenate([in_cells[pair], norm], axis=1)
        row = lax.broadcasted_iota(jnp.int32, full.shape, 0)
        for h in (2 * pair, 2 * pair + 1):
            own = (row >= KEY_DIM) if h % 2 else (row < KEY_DIM)
            high, low = split(jnp.where(own, full, 0.0))
            enter_ref[0, h] = high
            enter_ref[1, h] = low
    ring.pump_to(PUMP_MIX)

    @pl.loop(0, blocks)
    def _(b):
        mix_block(
            heads, b, q_ref, out_gate_ref, head_gain_ref, top_ref, cum_ref, num_ref, den_ref,
            in_top, enter_ref, mixed_ref,
        )

    tile = 512 if width % 512 == 0 else width

    def product(chunk, piece, store):
        start = pl.multiple_of(chunk * rows + piece * step, step)
        left = mixed_ref[pl.ds(start, step), :]

        @pl.loop(0, width // tile)
        def _(j):
            cols = pl.ds(pl.multiple_of(j * tile, tile), tile)
            store(cols, mm(left, out_weight_ref[:, cols]))

    sent, landing = [], []
    done = 0
    for k in list(range(1, xs)) + [0]:
        to_x = lax.rem(at_x + k, xs)
        for s in range(pieces):
            span = pl.ds(s * step, step)

            def put_pair(cols, block, k=k, span=span):
                pair_out[k, span, cols] = block.astype(bf16)

            product(to_x * CORES + 1 - core, s, put_pair)
            copy = remote(
                pair_out.at[k, span], pair_in.at[k, span],
                pair_send.at[k, s], pair_recv.at[k, s], {"tp": partner},
            )
            copy.start()
            sent.append(copy)

            def put_own(cols, block, span=span):
                total[span, cols] = block.astype(bf16).astype(f32)

            product(to_x * CORES + core, s, put_own)
            copy.wait_recv()
            summed = total[span, :] + pair_in[k, span, :].astype(f32)
            if k == 0:
                total[span, :] = summed
            else:
                x_out[k - 1, span, :] = summed.astype(bf16)
                copy = remote(
                    x_out.at[k - 1, span], x_in.at[k - 1, span],
                    x_send.at[k, s], x_recv.at[k, s], {"tp": peers[k]},
                )
                copy.start()
                sent.append(copy)
                landing.append((s, copy))
    ring.pump_to(PUMP_REDUCED)

    def block(device, s):
        start = pl.multiple_of(HALO + device * rows + s * step, HALO)
        return normed_ref.at[pl.ds(start, step)]

    for s in range(pieces):
        span = pl.ds(s * step, step)
        for at, copy in landing:
            if at == s:
                copy.wait_recv()
        summed = total[span, :]
        for k in range(1, xs):
            summed = summed + x_in[k - 1, span, :].astype(f32)
        mixer_out = summed.astype(bf16).astype(f32)
        after = residual_ref[span, :].astype(f32) + rms_gain(mixer_out, cell_gain_ref[...])
        after = after.astype(bf16)
        after_ref[span, :] = after
        normed = rms_gain(after.astype(f32), ffn_gain_ref[...])
        start = pl.multiple_of(HALO + me * rows + s * step, HALO)
        normed_ref[pl.ds(start, step), :] = normed.astype(bf16)
        own = block(me, s)
        for k in range(1, xs):
            sent.append(remote(own, own, gx_send.at[k, s], gx_recv.at[k, s], {"tp": peers[k]}))
            sent[-1].start()
        sent.append(remote(own, own, gp_send.at[0, s], gp_recv.at[0, s], {"tp": partner}))
        sent[-1].start()
        ring.pump_to(PUMP_NORM[s])
    for s in range(pieces):
        for k in range(1, xs):
            came = block(sources[k], s)
            remote(came, came, gx_send.at[k, s], gx_recv.at[k, s], {"tp": peers[k]}).wait_recv()
            sent.append(remote(came, came, gp_send.at[k, s], gp_recv.at[k, s], {"tp": partner}))
            sent[-1].start()
        ring.pump_to(PUMP_GATHER[s])
    for s in range(pieces):
        for k in range(xs):
            came = block(sources[k] + partner - me, s)
            remote(came, came, gp_send.at[k, s], gp_recv.at[k, s], {"tp": partner}).wait_recv()

    ahead, behind = lax.rem(sp + 1, sps), lax.rem(sp + sps - 1, sps)
    tail = normed_ref.at[pl.ds(tok_rows, HALO)]
    head = normed_ref.at[pl.ds(0, HALO)]

    @pl.when(sp + 1 < sps)
    def _():
        remote(tail, head, h_sems.at[0], h_sems.at[1], {"sp": ahead}).start()

    @pl.when(sp == 0)
    def _():
        normed_ref[pl.ds(0, HALO), :] = jnp.zeros((HALO, width), bf16)

    ring.pump_to(PUMP_UP)
    own_up.wait()
    ring.arrived_all("up")

    @pl.when(sp > 0)
    def _():
        remote(tail, head, h_sems.at[0], h_sems.at[1], {"sp": behind}).wait_recv()

    tiles, half = up_own.shape[0], up_own.shape[2] // 2

    def up_tile(j, cols):
        lift_ref[...] = mm(normed_ref[...], up_all[j]).astype(bf16).astype(f32)
        sums = []
        for taps, side in ((gate_taps_ref, 0), (value_taps_ref, 1)):
            summed = jnp.zeros((tok_rows, half), f32)
            for offset in range(WIDTH):
                tap = taps[offset : offset + 1, cols].astype(f32)
                at = pl.ds(HALO - WIDTH + 1 + offset, tok_rows)
                summed = summed + tap * lift_ref[at, pl.ds(side * half, half)]
            sums.append(summed)
        active_ref[:, cols] = (jax.nn.gelu(sums[0], approximate=True) * sums[1]).astype(bf16)

    if half % LANES == 0:
        edges = [tiles * i // len(PUMP_TILES) for i in range(len(PUMP_TILES) + 1)]
        for i, number in enumerate(PUMP_TILES):

            @pl.loop(edges[i], edges[i + 1])
            def _(j):
                up_tile(j, pl.ds(pl.multiple_of(j * half, half), half))

            ring.pump_to(number)
    else:
        for j in range(tiles):
            up_tile(j, pl.ds(j * half, half))

    own_down.wait()

    def close_columns(shard, slot):
        copies = []
        weight = down_all[shard]
        order = list(range(1, xs)) + [0]
        for k in order:
            chunk = lax.rem(at_x + k, xs) * CORES + 1 - core
            left = active_ref[pl.ds(pl.multiple_of(chunk * rows, rows), rows), :]
            pair_out2[shard, k] = mm(left, weight).astype(bf16)
            copy = remote(
                pair_out2.at[shard, k], pair_in2.at[shard, k],
                p2_send.at[slot, k], p2_recv.at[slot, k], {"tp": partner},
            )
            copy.start()
            copies.append(copy)
        for at, k in enumerate(order):
            chunk = lax.rem(at_x + k, xs) * CORES + core
            left = active_ref[pl.ds(pl.multiple_of(chunk * rows, rows), rows), :]
            part = mm(left, weight).astype(bf16).astype(f32)
            copies[at].wait_recv()
            summed = part + pair_in2[shard, k].astype(f32)
            if k == 0:
                total2[shard] = summed
            else:
                x_out2[shard, k - 1] = summed.astype(bf16)
                copy = remote(
                    x_out2.at[shard, k - 1], x_in2.at[shard, k - 1],
                    x2_send.at[slot, k], x2_recv.at[slot, k], {"tp": peers[k]},
                )
                copy.start()
                final.append(copy)
        sent.extend(copies)

    final = []
    close_columns(sp, 0)
    slot = 1
    for hop in range(1, sps // 2 + 1):
        for way in range(2):
            if hop == sps // 2 and way == 1:
                continue
            for event in ring.events[way]:
                if event[0] == "down" and event[3] == hop:
                    ring.arrived(way, event)
            if hop == sps // 2:
                for event in ring.events[1]:
                    if event[0] == "down" and event[3] == hop:
                        ring.arrived(1, event)
            if way == 0 or hop == sps // 2:
                ring.pump(1)
            close_columns(ring.shard(way, hop), slot)
            slot += 1
            ring.pump(1)
    ring.pump(len(ring.events[0]))
    for copy in final:
        copy.wait_recv()
    square = jnp.zeros((rows, 1), f32)
    for n in range(sps):
        summed = total2[n]
        for k in range(1, xs):
            summed = summed + x_in2[n, k - 1].astype(f32)
        summed = summed.astype(bf16).astype(f32)
        total2[n] = summed
        square = square + jnp.sum(summed * summed, axis=-1, keepdims=True)
    scale = rms_scale(square, width)
    part = width // sps
    for n in range(sps):
        cols = slice(n * part, (n + 1) * part)
        result = after_ref[:, cols].astype(f32) + total2[n] * scale * close_gain_ref[:, cols]
        out_ref[:, cols] = result.astype(bf16)
    for copy in sent + final + ring.sent:
        copy.wait_send()
    for d in range(1, sps):

        @pl.when(sp + d < sps)
        def _(d=d):
            ahead = {"sp": lax.rem(sp + d, sps)}
            remote(small_out, small_in.at[d], t_send.at[d], t_recv.at[d], ahead).wait_send()
            remote(cells_out, cells_in.at[d], s_send.at[d], s_recv.at[d], ahead).wait_send()

    @pl.when(sp + 1 < sps)
    def _():
        remote(tail, head, h_sems.at[0], h_sems.at[1], {"sp": ahead}).wait_send()


PUMP_START = 4
PUMP_STATE = 5
PUMP_MIX = 7
PUMP_REDUCED = 9
PUMP_NORM = (10, 10)
PUMP_GATHER = (11, 12)
PUMP_UP = 16
PUMP_TILES = (16, 17, 18, 19)


def shards(
    queries,
    keys,
    values,
    output_gate_logits,
    log_input_gate,
    forget_gate_logits,
    extra_forget_terms,
    per_head_norm_gain,
    output_weight,
    residual,
    after_cell_norm_gain,
    feedforward_norm_gain,
    closing_norm_gain,
    gate_up_weight,
    value_up_weight,
    gate_filter_taps,
    value_filter_taps,
    down_weight,
):
    count, sps = lax.axis_size("tp"), lax.axis_size("sp")
    xs = count // CORES
    tok_rows = queries.shape[0]
    heads = log_input_gate.shape[0]
    own_depth, hidden = gate_up_weight.shape
    width = output_weight.shape[1]
    own_width = down_weight.shape[1]
    rows = tok_rows // count
    pieces = 2
    half = LANES if hidden % LANES == 0 else LANES // 2
    tiles = hidden // half
    up_own = jnp.concatenate(
        [
            gate_up_weight.reshape(own_depth, tiles, half),
            value_up_weight.reshape(own_depth, tiles, half),
        ],
        axis=2,
    ).transpose(1, 0, 2)
    events = len(ring_events(sps)[0])
    vmem = pl.BlockSpec(memory_space=pltpu.VMEM)
    hbm = pl.BlockSpec(memory_space=pl.ANY)
    dma = pltpu.SemaphoreType.DMA
    V = pltpu.VMEM
    small = -(-(heads // 2 + 2 * heads) // 8) * 8
    pairs = heads // 2
    return pl.pallas_call(
        functools.partial(step_kernel, count, sps, pieces),
        out_shape=jax.ShapeDtypeStruct(residual.shape, bf16),
        in_specs=[vmem] * 13 + [hbm, vmem, vmem, hbm],
        out_specs=vmem,
        scratch_shapes=[
            V((tiles, own_depth * sps, 2 * half), bf16),
            V((sps, hidden, own_width), bf16),
            V((8, tok_rows), f32),
            V((8, tok_rows), f32),
            V((8, tok_rows), f32),
            V((tok_rows, heads * VAL_DIM), f32),
            V((tok_rows, heads * VAL_DIM), f32),
            V((heads, LANES, 2 * LANES), f32),
            V((8, LANES), f32),
            V((pairs, LANES, LANES), f32),
            V((small, LANES), f32),
            V((sps, pairs, LANES, LANES), f32),
            V((sps, small, LANES), f32),
            V((pairs, LANES, LANES), f32),
            V((8, LANES), f32),
            V((8, LANES), f32),
            V((8, LANES), f32),
            V((2, heads, LANES, 2 * LANES), bf16),
            V((tok_rows, heads * VAL_DIM), bf16),
            V((rows, width), f32),
            V((xs, rows, width), bf16),
            V((xs, rows, width), bf16),
            V((max(xs - 1, 1), rows, width), bf16),
            V((max(xs - 1, 1), rows, width), bf16),
            V((rows, width), bf16),
            V((HALO + tok_rows, width), bf16),
            V((HALO + tok_rows, 2 * half), f32),
            V((tok_rows, hidden), bf16),
            V((sps, rows, own_width), f32),
            V((sps, xs, rows, own_width), bf16),
            V((sps, xs, rows, own_width), bf16),
            V((sps, max(xs - 1, 1), rows, own_width), bf16),
            V((sps, max(xs - 1, 1), rows, own_width), bf16),
            dma((2, events)),
            dma((2, events)),
            dma((2,)),
            dma((sps,)),
            dma((sps,)),
            dma((sps,)),
            dma((sps,)),
            dma((2,)),
        ]
        + [dma((xs, pieces))] * 8
        + [dma((sps, xs))] * 4,
        compiler_params=pltpu.CompilerParams(
            collective_id=0, has_side_effects=True, vmem_limit_bytes=VMEM_BYTES
        ),
        cost_estimate=pl.CostEstimate(
            flops=6 * tok_rows * hidden * width, bytes_accessed=3 * 10**7, transcendentals=0
        ),
        name="step",
    )(
        queries, keys, values, output_gate_logits, log_input_gate, forget_gate_logits,
        extra_forget_terms, per_head_norm_gain.reshape(1, -1), output_weight, residual,
        after_cell_norm_gain.reshape(1, -1), feedforward_norm_gain.reshape(1, -1),
        closing_norm_gain.reshape(1, -1), up_own, gate_filter_taps, value_filter_taps, down_weight,
    )


def solution(mesh):
    placed = (
        P("sp", "tp"),
        P("sp", "tp"),
        P("sp", "tp"),
        P("sp", "tp"),
        P("tp", "sp"),
        P("tp", "sp"),
        P("tp", "sp"),
        P("tp"),
        P("tp", None),
        P(("sp", "tp"), None),
        P(),
        P(),
        P(),
        P("sp", "tp"),
        P("sp", "tp"),
        P(None, "tp"),
        P(None, "tp"),
        P("tp", "sp"),
    )
    return jax.shard_map(
        shards, mesh=mesh, in_specs=placed, out_specs=P(("sp", "tp"), None), check_vma=False
    )
```

profile of v0, /device:TPU:24, one launch (start us, length us, event | category | flops | bytes accessed | tf_op | source)
XLA Modules:
  0.0 220.1 jit_solution(14226213058031292065)
XLA Ops:
  0.0 0.0 copy-start
  0.0 1.4 copy.19
  1.5 0.3 copy.21
  1.8 0.0 copy-done
  1.8 0.3 copy.20
  2.1 0.3 copy.22
  2.4 1.3 maximum_bitcast_fusion.up_own
  3.8 214.1 %step.1 = bf16[256,2048]{1,0:T(8,128)(2,1)} custom-call(bf16[1024,256]{1,0:T(8,128)(2,1)} %q_ref.1, bf16[1024,256]{1,0:T(8,128)(2,1)} %k_ref.1, bf16[1024,512]{1,0:T(8,128)(2,1)} %v_ref.1, bf16[1024,512]{1,0:T(8,128)(2,1)} %out_gate_ref.1, f32[4,1024]{1,0:T(4,128)} %in_gate_ref.1, f32[4,1024]{1,0:T(4,128)} %forget_ref.1, f32[4,1024]{1,0:T(4,128)} %extra_ref.1, ...), custom_call_target="tpu_custom_call" | custom-call | flops 17716740096 | bytes 30000000 | tf_op jit(solution)/shard_map/step/pallas_call | solution.py:686
  217.8 2.3 %copy.24 = bf16[256,2048]{1,0:T(8,128)(2,1)} copy(bf16[256,2048]{1,0:T(8,128)(2,1)} %step.1) | data formatting | bytes 2097152
Async XLA Ops:
  0.0 1.8 copy-start
where the time goes:
time: 220 us
  Pallas kernels  214 us (97%)
  local copies, waits for them, and re-layouts  4.73 us (2%)
    pallas_call x1, Pallas kernels, shards(): pl.pallas_call(functools.partial(step_kernel, count, sps, pieces), out_sh...  214 us

commit v1 on v0

--- a/solution.py
+++ b/solution.py
@@ -638,7 +638,7 @@
 PUMP_TILES = (16, 17, 18, 19)
 
 
-def shards(
+def ring_shards(
     queries,
     keys,
     values,
@@ -748,6 +748,747 @@
     )
 
 
+class Line:
+    def __init__(self, rows_z, up_own, up_all, down_own, down_all, y_send, y_recv, send, recv):
+        self.rows_z = rows_z
+        self.up_own, self.up_all = up_own, up_all
+        self.down_own, self.down_all = down_own, down_all
+        self.y_send, self.y_recv, self.send, self.recv = y_send, y_recv, send, recv
+        self.sp = lax.axis_index("sp")
+        self.z, self.y = self.sp // 2, lax.rem(self.sp, 2)
+        self.units = [("up", yy, r) for yy in range(2) for r in range(2)]
+        self.units += [("down", yy, 0) for yy in range(2)]
+        self.events = [
+            (unit, hop)
+            for kind in ("up", "down")
+            for hop in range(1, rows_z)
+            for unit in self.units
+            if unit[0] == kind
+        ]
+        self.waited = set()
+        self.next = 0
+
+    def piece(self, unit, z, y):
+        kind, _, r = unit
+        shard = z * 2 + y
+        if kind == "down":
+            return self.down_all.at[shard]
+        rows = self.up_own.shape[1]
+        start = pl.multiple_of(shard * rows + r * (rows // 2), rows // 2)
+        return self.up_all.at[pl.ds(start, rows // 2)]
+
+    def own(self, unit, y):
+        kind, _, r = unit
+        if kind == "down":
+            rows = self.down_all.shape[1]
+            return self.down_own.at[pl.ds(pl.multiple_of(y * rows, rows), rows)]
+        rows = self.up_own.shape[1]
+        return self.up_own.at[y, pl.ds(r * (rows // 2), rows // 2)]
+
+    def side(self, yy):
+        return self.y if yy == 0 else 1 - self.y
+
+    def across(self, unit):
+        at = self.units.index(("down" if unit[0] == "down" else "up", 1, unit[2]))
+        return remote(
+            self.own(unit, 1 - self.y), self.piece(unit, self.z, self.y),
+            self.y_send.at[at], self.y_recv.at[at], {"sp": self.z * 2 + 1 - self.y},
+        )
+
+    def start_across(self):
+        for unit in self.units:
+            if unit[1] == 1:
+                self.across(unit).start()
+
+    def came_across(self, unit):
+        if unit in self.waited:
+            return
+        self.waited.add(unit)
+        at = self.units.index(unit)
+        came = self.piece(unit, self.z, 1 - self.y)
+        remote(
+            came, came, self.y_send.at[at], self.y_recv.at[at], {"sp": self.z * 2 + 1 - self.y}
+        ).wait_recv()
+
+    def valid(self, way, hop):
+        return self.z - hop >= 0 if way == 0 else self.z + hop < self.rows_z
+
+    def origin(self, way, hop):
+        return self.z - hop if way == 0 else self.z + hop
+
+    def onward(self, way):
+        return lax.rem(self.z + (1 if way == 0 else self.rows_z - 1), self.rows_z)
+
+    def sends(self, way, hop):
+        onward = self.z + 1 < self.rows_z if way == 0 else self.z >= 1
+        return jnp.logical_and(onward, self.valid(way, hop - 1))
+
+    def copy(self, way, event):
+        unit, hop = event
+        at = self.events.index(event)
+        y = self.side(unit[1])
+        dst = self.piece(unit, self.origin(way, hop - 1), y)
+        src = self.own(unit, self.y) if hop == 1 and unit[1] == 0 else dst
+        target = {"sp": self.onward(way) * 2 + self.y}
+        return remote(src, dst, self.send.at[way, at], self.recv.at[way, at], target)
+
+    def arrived(self, way, event):
+        if (way, event) in self.waited:
+            return
+        self.waited.add((way, event))
+        unit, hop = event
+        at = self.events.index(event)
+
+        @pl.when(self.valid(way, hop))
+        def _():
+            came = self.piece(unit, self.origin(way, hop), self.side(unit[1]))
+            where = {"sp": self.onward(1 - way) * 2 + self.y}
+            remote(came, came, self.send.at[way, at], self.recv.at[way, at], where).wait_recv()
+
+    def pump_to(self, number):
+        while self.next < min(number, len(self.events)):
+            event = self.events[self.next]
+            unit, hop = event
+            if hop == 1 and unit[1] == 1:
+                self.came_across(unit)
+            for way in range(2):
+                if hop > 1:
+                    self.arrived(way, (unit, hop - 1))
+
+                @pl.when(self.sends(way, hop))
+                def _(way=way, event=event):
+                    self.copy(way, event).start()
+
+            self.next += 1
+
+    def arrived_all(self, kind):
+        for unit in self.units:
+            if unit[0] == kind and unit[1] == 1:
+                self.came_across(unit)
+        for event in self.events:
+            if event[0][0] == kind:
+                for way in range(2):
+                    self.arrived(way, event)
+
+    def wait_sends(self):
+        for unit in self.units:
+            if unit[1] == 1:
+                self.across(unit).wait_send()
+        for event in self.events:
+            for way in range(2):
+
+                @pl.when(self.sends(way, event[1]))
+                def _(way=way, event=event):
+                    self.copy(way, event).wait_send()
+
+
+def clear_state(in_cells, in_norm, in_top, in_after):
+    in_cells[...] = jnp.zeros_like(in_cells)
+    in_norm[...] = jnp.zeros_like(in_norm)
+    in_top[...] = jnp.full_like(in_top, empty_log)
+    in_after[...] = jnp.zeros_like(in_after)
+
+
+def total_square(array):
+    return jnp.sum(jnp.sum(array * array, axis=2, keepdims=True), axis=0, keepdims=True)
+
+
+def plane_kernel(
+    count, sps, pieces,
+    q_ref, k_ref, v_ref, out_gate_ref, in_gate_ref, forget_ref, extra_ref, head_gain_ref,
+    out_weight_ref, residual_ref, cell_gain_ref, ffn_gain_ref, close_gain_ref,
+    up_own, gate_taps_ref, value_taps_ref, down_own,
+    out_ref,
+    up_all, down_all,
+    reach_ref, top_ref, cum_ref, num_ref, den_ref, state_ref, held_ref,
+    y_cells, y_small, z_cells, z_small, p_cells, p_small,
+    in_cells, in_norm, in_top, in_after, enter_ref,
+    mixed_ref, total, pair_out, pair_in, one_out, one_in, two_out, two_in,
+    after_ref, normed_ref, lift_ref, active_ref,
+    wy_send, wy_recv, wz_send, wz_recv, own_sems,
+    sy_send, sy_recv, sz_send, sz_recv, h_sems,
+    pair_send, pair_recv, x_send, x_recv,
+    ax_send, ax_recv, ay_send, ay_recv, ad_send, ad_recv, gp_send, gp_recv,
+    p2_send, p2_recv, one_send, one_recv, two_send, two_recv,
+):
+    sp = lax.axis_index("sp")
+    me = lax.axis_index("tp")
+    z, y = sp // 2, lax.rem(sp, 2)
+    x, core = me // CORES, lax.rem(me, CORES)
+    rows_z = sps // 2
+    partner, x_peer = {"tp": x * CORES + 1 - core}, {"tp": (1 - x) * CORES + core}
+    y_peer = {"sp": z * 2 + 1 - y}
+    tok_rows, heads = q_ref.shape[0], in_gate_ref.shape[0]
+    blocks = tok_rows // CHUNK
+    rows = tok_rows // count
+    step = rows // pieces
+    width = out_weight_ref.shape[1]
+    cw = width // sps
+    pairs = heads // 2
+    line = Line(
+        rows_z, up_own, up_all, down_own, down_all, wy_send, wy_recv, wz_send, wz_recv
+    )
+
+    barrier = pltpu.get_barrier_semaphore()
+    friends = [partner, x_peer, y_peer]
+    friends += [{"sp": lax.rem(z + d, rows_z) * 2 + y} for d in range(1, rows_z)]
+    for where in friends:
+        pl.semaphore_signal(barrier, inc=1, device_id=where, device_id_type=MESH)
+    pl.semaphore_wait(barrier, len(friends))
+
+    line.start_across()
+    line.pump_to(LINE_START)
+    own_rows = up_own.shape[1]
+    own_up = pltpu.make_async_copy(
+        up_own.at[y],
+        up_all.at[pl.ds(pl.multiple_of(sp * own_rows, own_rows), own_rows)],
+        own_sems.at[0],
+    )
+    own_up.start()
+    own_down = pltpu.make_async_copy(
+        line.own(("down", 0, 0), y), down_all.at[sp], own_sems.at[1]
+    )
+    own_down.start()
+
+    gate_rows_into(heads, in_gate_ref, forget_ref, extra_ref, reach_ref, top_ref, cum_ref)
+    state_ref[...] = jnp.zeros_like(state_ref)
+    held_ref[...] = jnp.full_like(held_ref, empty_log)
+
+    @pl.loop(0, blocks)
+    def _(b):
+        cell_block(
+            heads, b, q_ref, k_ref, v_ref, reach_ref, top_ref, num_ref, den_ref, state_ref, held_ref
+        )
+
+    last = cum_ref[:, pl.ds(tok_rows - LANES, LANES)]
+    cum_last = jnp.broadcast_to(last[:, LANES - 1 :], last.shape)
+    pack_state(heads, state_ref, held_ref, cum_last, y_cells.at[y], y_small.at[y])
+
+    def swap(array, side, at):
+        return remote(array.at[side], array.at[side], sy_send.at[at], sy_recv.at[at], y_peer)
+
+    swap(y_small, y, 0).start()
+    swap(y_cells, y, 1).start()
+    swap(y_small, 1 - y, 0).wait_recv()
+    swap(y_cells, 1 - y, 1).wait_recv()
+    acc = (in_cells, in_norm, in_top, in_after)
+    clear_state(*acc)
+    merge_state(heads, y_cells.at[1], y_small.at[1], *acc)
+    merge_state(heads, y_cells.at[0], y_small.at[0], *acc)
+    p_cells[...] = in_cells[...]
+    p_small[...] = jnp.concatenate(
+        [
+            in_norm[0:pairs, :], in_top[0:heads, :], in_after[0:heads, :],
+            jnp.zeros((p_small.shape[0] - pairs - 2 * heads, LANES), f32),
+        ],
+        axis=0,
+    )
+
+    def along(d):
+        where = {"sp": lax.rem(z + d, rows_z) * 2 + y}
+        return (
+            remote(p_small, z_small.at[d], sz_send.at[0, d], sz_recv.at[0, d], where),
+            remote(p_cells, z_cells.at[d], sz_send.at[1, d], sz_recv.at[1, d], where),
+        )
+
+    for d in range(1, rows_z):
+
+        @pl.when(z + d < rows_z)
+        def _(d=d):
+            for copy in along(d):
+                copy.start()
+
+    line.pump_to(LINE_STATE)
+    clear_state(*acc)
+
+    @pl.when(y == 1)
+    def _():
+        merge_state(heads, y_cells.at[0], y_small.at[0], *acc)
+
+    for d in range(1, rows_z):
+
+        @pl.when(z - d >= 0)
+        def _(d=d):
+            for copy in along(d):
+                copy.wait_recv()
+            merge_state(heads, z_cells.at[d], z_small.at[d], *acc)
+
+    for pair in range(pairs):
+        norm = jnp.broadcast_to(in_norm[pair : pair + 1, :], (LANES, LANES)).T
+        full = jnp.concatenate([in_cells[pair], norm], axis=1)
+        row = lax.broadcasted_iota(jnp.int32, full.shape, 0)
+        for h in (2 * pair, 2 * pair + 1):
+            own = (row >= KEY_DIM) if h % 2 else (row < KEY_DIM)
+            high, low = split(jnp.where(own, full, 0.0))
+            enter_ref[0, h] = high
+            enter_ref[1, h] = low
+    line.pump_to(LINE_MIX)
+
+    @pl.loop(0, blocks)
+    def _(b):
+        mix_block(
+            heads, b, q_ref, out_gate_ref, head_gain_ref, top_ref, cum_ref, num_ref, den_ref,
+            in_top, enter_ref, mixed_ref,
+        )
+
+    def product(chunk, piece, store):
+        start = pl.multiple_of(chunk * rows + piece * step, step)
+        left = mixed_ref[pl.ds(start, step), :]
+
+        @pl.loop(0, sps)
+        def _(j):
+            cols = pl.ds(pl.multiple_of(j * cw, cw), cw)
+            store(j, mm(left, out_weight_ref[:, cols]))
+
+    sent, landing = [], []
+    for k in (1, 0):
+        to_x = x if k == 0 else 1 - x
+        for s in range(pieces):
+            span = pl.ds(s * step, step)
+
+            def put_pair(j, block, k=k, span=span):
+                pair_out[j, k, span, :] = block.astype(bf16)
+
+            product(to_x * CORES + 1 - core, s, put_pair)
+            copy = remote(
+                pair_out.at[:, k, span], pair_in.at[:, k, span],
+                pair_send.at[k, s], pair_recv.at[k, s], partner,
+            )
+            copy.start()
+            sent.append(copy)
+
+            def put_own(j, block, span=span):
+                total[j, span, :] = block.astype(bf16).astype(f32)
+
+            product(to_x * CORES + core, s, put_own)
+            copy.wait_recv()
+            summed = total[:, span, :] + pair_in[:, k, span, :].astype(f32)
+            if k == 0:
+                total[:, span, :] = summed
+            else:
+                one_out[:, s] = summed.astype(bf16)
+                copy = remote(
+                    one_out.at[:, s], one_in.at[:, s], x_send.at[s], x_recv.at[s], x_peer
+                )
+                copy.start()
+                sent.append(copy)
+                landing.append(copy)
+    line.pump_to(LINE_REDUCED)
+
+    def block(side, owner, s):
+        start = pl.multiple_of(HALO + side * tok_rows + owner * rows + s * step, HALO)
+        return normed_ref.at[pl.ds(start, step)]
+
+    def give(array, sems, at, where):
+        copy = remote(array, array, sems[0].at[at], sems[1].at[at], where)
+        copy.start()
+        sent.append(copy)
+
+    def take(array, sems, at, where):
+        remote(array, array, sems[0].at[at], sems[1].at[at], where).wait_recv()
+
+    to_x, to_y, to_d = (ax_send, ax_recv), (ay_send, ay_recv), (ad_send, ad_recv)
+    to_p = (gp_send, gp_recv)
+    other = (1 - x) * CORES + core
+    for s in range(pieces):
+        span = pl.ds(s * step, step)
+        landing[s].wait_recv()
+        summed = total[:, span, :] + one_in[:, s].astype(f32)
+        mixer_out = summed.astype(bf16).astype(f32)
+        scale = rms_scale(total_square(mixer_out), width)
+        held = []
+        for j in range(sps):
+            cols = slice(j * cw, (j + 1) * cw)
+            after = residual_ref[span, cols].astype(f32) + (
+                mixer_out[j] * scale[0] * cell_gain_ref[:, cols]
+            )
+            after = after.astype(bf16)
+            after_ref[j, span, :] = after
+            held.append(after.astype(f32))
+        square = sum(jnp.sum(a * a, axis=-1, keepdims=True) for a in held)
+        scale = rms_scale(square, width)
+        start = pl.multiple_of(HALO + y * tok_rows + me * rows + s * step, HALO)
+        for j in range(sps):
+            cols = slice(j * cw, (j + 1) * cw)
+            normed_ref[pl.ds(start, step), cols] = (
+                held[j] * scale * ffn_gain_ref[:, cols]
+            ).astype(bf16)
+        own = block(y, me, s)
+        give(own, to_y, s, y_peer)
+        give(own, to_x, s, x_peer)
+        give(own, to_p, s, partner)
+        line.pump_to(LINE_NORM[s])
+    for s in range(pieces):
+        from_x, from_y = block(y, other, s), block(1 - y, me, s)
+        if s == 0:
+            take(from_y, to_y, s, y_peer)
+            give(from_y, to_d, s, x_peer)
+            give(from_y, to_p, 2 * pieces + s, partner)
+            take(from_x, to_x, s, x_peer)
+            give(from_x, to_p, pieces + s, partner)
+        else:
+            take(from_x, to_x, s, x_peer)
+            give(from_x, to_d, s, y_peer)
+            give(from_x, to_p, pieces + s, partner)
+            take(from_y, to_y, s, y_peer)
+            give(from_y, to_p, 2 * pieces + s, partner)
+        line.pump_to(LINE_GATHER[s])
+    for s in range(pieces):
+        from_d = block(1 - y, other, s)
+        take(from_d, to_d, s, x_peer if s == 0 else y_peer)
+        give(from_d, to_p, 3 * pieces + s, partner)
+    mate, other_mate = x * CORES + 1 - core, (1 - x) * CORES + 1 - core
+    for s in range(pieces):
+        take(block(y, mate, s), to_p, s, partner)
+        take(block(y, other_mate, s), to_p, pieces + s, partner)
+        take(block(1 - y, mate, s), to_p, 2 * pieces + s, partner)
+        take(block(1 - y, other_mate, s), to_p, 3 * pieces + s, partner)
+
+    group = 2 * tok_rows
+
+    def halo(plane):
+        return remote(
+            normed_ref.at[pl.ds(group, HALO)], normed_ref.at[pl.ds(0, HALO)],
+            h_sems.at[0], h_sems.at[1], {"sp": lax.rem(plane, rows_z) * 2 + y},
+        )
+
+    @pl.when(z + 1 < rows_z)
+    def _():
+        halo(z + 1).start()
+
+    @pl.when(z == 0)
+    def _():
+        normed_ref[pl.ds(0, HALO), :] = jnp.zeros((HALO, width), bf16)
+
+    line.pump_to(LINE_UP)
+    own_up.wait()
+    line.arrived_all("up")
+
+    @pl.when(z > 0)
+    def _():
+        halo(z + rows_z - 1).wait_recv()
+
+    hidden = active_ref.shape[1]
+    full, rest = hidden // LANES, hidden % LANES
+
+    def up_tile(weight_cols, cols, half):
+        lift_ref[:, pl.ds(0, 2 * half)] = (
+            mm(normed_ref[...], up_all[:, weight_cols]).astype(bf16).astype(f32)
+        )
+
+        @pl.loop(0, group // CONV_ROWS)
+        def _(i):
+            sums = []
+            for taps, side in ((gate_taps_ref, 0), (value_taps_ref, 1)):
+                summed = jnp.zeros((CONV_ROWS, half), f32)
+                base = pl.multiple_of(i * CONV_ROWS, CONV_ROWS)
+                window = lift_ref[pl.ds(base, CONV_ROWS + HALO), pl.ds(side * half, half)]
+                for offset in range(WIDTH):
+                    tap = taps[y, offset : offset + 1, cols].astype(f32)
+                    low = HALO - WIDTH + 1 + offset
+                    summed = summed + tap * window[low : low + CONV_ROWS]
+                sums.append(summed)
+            active = jax.nn.gelu(sums[0], approximate=True) * sums[1]
+            active_ref[pl.ds(base, CONV_ROWS), cols] = active.astype(bf16)
+
+    edges = [full * i // len(LINE_TILES) for i in range(len(LINE_TILES) + 1)]
+    for i, number in enumerate(LINE_TILES):
+
+        @pl.loop(edges[i], edges[i + 1])
+        def _(j):
+            up_tile(
+                pl.ds(pl.multiple_of(j * 2 * LANES, 2 * LANES), 2 * LANES),
+                pl.ds(pl.multiple_of(j * LANES, LANES), LANES),
+                LANES,
+            )
+
+        line.pump_to(number)
+    if rest:
+        up_tile(pl.ds(full * 2 * LANES, 2 * rest), pl.ds(full * LANES, rest), rest)
+
+    own_down.wait()
+    for copy in sent:
+        copy.wait_send()
+
+    def chunk_rows(side, at_x, at_core):
+        start = side * tok_rows + (at_x * CORES + at_core) * rows
+        return pl.ds(pl.multiple_of(start, rows), rows)
+
+    sides = ((1 - y, 1 - x), (y, 1 - x), (1 - y, x), (y, x))
+
+    def pair_copy(shard, k):
+        return remote(
+            pair_out.at[shard, k], pair_in.at[shard, k],
+            p2_send.at[shard, k], p2_recv.at[shard, k], partner,
+        )
+
+    def one_copy(shard, at):
+        return remote(
+            one_out.at[shard, at], one_in.at[shard, at],
+            one_send.at[shard, at], one_recv.at[shard, at], x_peer if at < 2 else y_peer,
+        )
+
+    def two_copy(shard, at):
+        return remote(
+            two_out.at[shard, at], two_in.at[shard, at],
+            two_send.at[shard, at], two_recv.at[shard, at], y_peer if at == 0 else x_peer,
+        )
+
+    low, high = slice(0, step), slice(step, rows)
+
+    def multiply(shard):
+        weight = down_all[shard]
+        for k, (side, at_x) in enumerate(sides):
+            left = active_ref[chunk_rows(side, at_x, 1 - core), :]
+            pair_out[shard, k] = mm(left, weight).astype(bf16)
+            pair_copy(shard, k).start()
+        for k, (side, at_x) in enumerate(sides):
+            left = active_ref[chunk_rows(side, at_x, core), :]
+            part = mm(left, weight).astype(bf16).astype(f32)
+            pair_copy(shard, k).wait_recv()
+            summed = part + pair_in[shard, k].astype(f32)
+            if k == 0:
+                one_out[shard, 0] = summed[low].astype(bf16)
+                one_copy(shard, 0).start()
+                one_out[shard, 2] = summed[high].astype(bf16)
+                one_copy(shard, 2).start()
+            elif k == 1:
+                one_out[shard, 1] = summed[low].astype(bf16)
+                one_copy(shard, 1).start()
+                two_out[shard, 1] = summed[high].astype(bf16)
+            elif k == 2:
+                one_out[shard, 3] = summed[high].astype(bf16)
+                one_copy(shard, 3).start()
+                two_out[shard, 0] = summed[low].astype(bf16)
+            else:
+                total[shard] = summed
+
+    def pass_on(shard):
+        one_copy(shard, 0).wait_recv()
+        summed = two_out[shard, 0].astype(f32) + one_in[shard, 0].astype(f32)
+        two_out[shard, 0] = summed.astype(bf16)
+        two_copy(shard, 0).start()
+        one_copy(shard, 2).wait_recv()
+        summed = two_out[shard, 1].astype(f32) + one_in[shard, 2].astype(f32)
+        two_out[shard, 1] = summed.astype(bf16)
+        two_copy(shard, 1).start()
+        one_copy(shard, 1).wait_recv()
+        one_copy(shard, 3).wait_recv()
+
+    steps = [(None, 0, 0), (None, 0, 1)]
+    for hop in range(1, rows_z):
+        for yy in range(2):
+            for way in range(2):
+                steps.append((way, hop, yy))
+
+    def shard_of(way, hop, yy):
+        return (z if way is None else line.origin(way, hop)) * 2 + line.side(yy)
+
+    def at_step(entry, action):
+        way, hop, yy = entry
+        if way is None:
+            action()
+        else:
+            pl.when(line.valid(way, hop))(action)
+
+    first_down = 4 * (rows_z - 1)
+    waiting = []
+    for way, hop, yy in steps:
+        unit = ("down", yy, 0)
+        if way is None:
+            if yy:
+                line.came_across(unit)
+        else:
+            line.pump_to(first_down + 2 * hop + yy + 1)
+            line.arrived(way, (unit, hop))
+        entry = (way, hop, yy)
+        shard = shard_of(way, hop, yy)
+        at_step(entry, functools.partial(multiply, shard))
+        waiting.append((entry, shard))
+        if len(waiting) > 2:
+            entry, shard = waiting.pop(0)
+            at_step(entry, functools.partial(pass_on, shard))
+    for entry, shard in waiting:
+        at_step(entry, functools.partial(pass_on, shard))
+    for entry in steps:
+
+        def finish(entry=entry):
+            shard = shard_of(*entry)
+            two_copy(shard, 0).wait_recv()
+            two_copy(shard, 1).wait_recv()
+            total[shard, low] = (
+                total[shard, low] + one_in[shard, 1].astype(f32) + two_in[shard, 0].astype(f32)
+            )
+            total[shard, high] = (
+                total[shard, high] + one_in[shard, 3].astype(f32) + two_in[shard, 1].astype(f32)
+            )
+
+        at_step(entry, finish)
+    summed = total[...].astype(bf16).astype(f32)
+    scale = rms_scale(total_square(summed), width)
+    for j in range(sps):
+        cols = slice(j * cw, (j + 1) * cw)
+        result = after_ref[j].astype(f32) + summed[j] * scale[0] * close_gain_ref[:, cols]
+        out_ref[:, cols] = result.astype(bf16)
+
+    for entry in steps:
+
+        def sends_done(entry=entry):
+            shard = shard_of(*entry)
+            for k in range(4):
+                pair_copy(shard, k).wait_send()
+                one_copy(shard, k).wait_send()
+            for k in range(2):
+                two_copy(shard, k).wait_send()
+
+        at_step(entry, sends_done)
+    line.wait_sends()
+    swap(y_small, y, 0).wait_send()
+    swap(y_cells, y, 1).wait_send()
+    for d in range(1, rows_z):
+
+        @pl.when(z + d < rows_z)
+        def _(d=d):
+            for copy in along(d):
+                copy.wait_send()
+
+    @pl.when(z + 1 < rows_z)
+    def _():
+        halo(z + 1).wait_send()
+
+
+LINE_START = 2
+LINE_STATE = 4
+LINE_MIX = 6
+LINE_REDUCED = 9
+LINE_NORM = (10, 10)
+LINE_GATHER = (11, 12)
+LINE_UP = 14
+LINE_TILES = (14, 14)
+CONV_ROWS = 256
+
+
+def by_side(array, axis):
+    shape = array.shape
+    parted = shape[:axis] + (2, shape[axis] // 2) + shape[axis + 1 :]
+    return jnp.moveaxis(array.reshape(parted), axis, 0)
+
+
+def plane_shards(
+    queries, keys, values, output_gate_logits, log_input_gate, forget_gate_logits,
+    extra_forget_terms, per_head_norm_gain, output_weight, residual, after_cell_norm_gain,
+    feedforward_norm_gain, closing_norm_gain, gate_up_weight, value_up_weight,
+    gate_filter_taps, value_filter_taps, down_weight,
+):
+    count, sps = lax.axis_size("tp"), lax.axis_size("sp")
+    rows_z = sps // 2
+    tok_rows = queries.shape[0]
+    heads = log_input_gate.shape[0]
+    own_depth = gate_up_weight.shape[0]
+    hidden = gate_up_weight.shape[1] // 2
+    width = output_weight.shape[1]
+    cw = down_weight.shape[1]
+    rows = tok_rows // count
+    pieces = 2
+    step = rows // pieces
+    gate_parts, value_parts = by_side(gate_up_weight, 1), by_side(value_up_weight, 1)
+    tiles = []
+    for start in range(0, hidden, LANES):
+        cols = slice(start, min(start + LANES, hidden))
+        tiles += [gate_parts[:, :, cols], value_parts[:, :, cols]]
+    up_own = jnp.concatenate(tiles, axis=2)
+    vmem = pl.BlockSpec(memory_space=pltpu.VMEM)
+    hbm = pl.BlockSpec(memory_space=pl.ANY)
+    dma = pltpu.SemaphoreType.DMA
+    V = pltpu.VMEM
+    pairs = heads // 2
+    small = -(-(pairs + 2 * heads) // 8) * 8
+    cells = (pairs, LANES, LANES)
+    return pl.pallas_call(
+        functools.partial(plane_kernel, count, sps, pieces),
+        out_shape=jax.ShapeDtypeStruct(residual.shape, bf16),
+        in_specs=[vmem] * 13 + [hbm, vmem, vmem, hbm],
+        out_specs=vmem,
+        scratch_shapes=[
+            V((own_depth * sps, 2 * hidden), bf16),
+            V((sps, hidden, cw), bf16),
+            V((8, tok_rows), f32),
+            V((8, tok_rows), f32),
+            V((8, tok_rows), f32),
+            V((tok_rows, heads * VAL_DIM), f32),
+            V((tok_rows, heads * VAL_DIM), f32),
+            V((heads, LANES, 2 * LANES), f32),
+            V((8, LANES), f32),
+            V((2,) + cells, f32),
+            V((2, small, LANES), f32),
+            V((rows_z,) + cells, f32),
+            V((rows_z, small, LANES), f32),
+            V(cells, f32),
+            V((small, LANES), f32),
+            V(cells, f32),
+            V((8, LANES), f32),
+            V((8, LANES), f32),
+            V((8, LANES), f32),
+            V((2, heads, LANES, 2 * LANES), bf16),
+            V((tok_rows, heads * VAL_DIM), bf16),
+            V((sps, rows, cw), f32),
+            V((sps, 4, rows, cw), bf16),
+            V((sps, 4, rows, cw), bf16),
+            V((sps, 4, step, cw), bf16),
+            V((sps, 4, step, cw), bf16),
+            V((sps, 2, step, cw), bf16),
+            V((sps, 2, step, cw), bf16),
+            V((sps, rows, cw), bf16),
+            V((HALO + 2 * tok_rows, width), bf16),
+            V((HALO + 2 * tok_rows, 2 * LANES), f32),
+            V((2 * tok_rows, hidden), bf16),
+            dma((6,)),
+            dma((6,)),
+            dma((2, 6 * (rows_z - 1))),
+            dma((2, 6 * (rows_z - 1))),
+            dma((2,)),
+            dma((2,)),
+            dma((2,)),
+            dma((2, rows_z)),
+            dma((2, rows_z)),
+            dma((2,)),
+            dma((2, pieces)),
+            dma((2, pieces)),
+            dma((pieces,)),
+            dma((pieces,)),
+        ]
+        + [dma((pieces,))] * 6
+        + [dma((4 * pieces,))] * 2
+        + [dma((sps, 4))] * 4
+        + [dma((sps, 2))] * 2,
+        compiler_params=pltpu.CompilerParams(
+            collective_id=0, has_side_effects=True, vmem_limit_bytes=VMEM_BYTES
+        ),
+        cost_estimate=pl.CostEstimate(
+            flops=12 * tok_rows * hidden * width, bytes_accessed=3 * 10**7, transcendentals=0
+        ),
+        name="plane",
+    )(
+        queries, keys, values, output_gate_logits, log_input_gate, forget_gate_logits,
+        extra_forget_terms, per_head_norm_gain.reshape(1, -1), output_weight, residual,
+        after_cell_norm_gain.reshape(1, -1), feedforward_norm_gain.reshape(1, -1),
+        closing_norm_gain.reshape(1, -1), up_own, by_side(gate_filter_taps, 1),
+        by_side(value_filter_taps, 1), down_weight,
+    )
+
+
+def shards(*arrays):
+    count, sps = lax.axis_size("tp"), lax.axis_size("sp")
+    hidden, own_width = arrays[17].shape
+    plane = (
+        grid_of(sps)[1] == 2
+        and count == 2 * CORES
+        and own_width % LANES == 0
+        and hidden % 32 == 0
+    )
+    return plane_shards(*arrays) if plane else ring_shards(*arrays)
+
+
 def solution(mesh):
     placed = (
         P("sp", "tp"),

time: 220 us -> 205 us (0.932)
  Pallas kernels: 214 us -> 196 us
  local copies, waits for them, and re-layouts: 4.73 us -> 9.03 us
    pallas_call x1, Pallas kernels: 214 us -> 196 us  [plane_shards(): pl.pallas_call(functools.partial(plane_kernel, count, sps, pieces), out_s...]
    concatenate x0 -> x1, local copies, waits for them, and re-layouts: none -> 3.28 us  [plane_shards(): up_own = jnp.concatenate(tiles, axis=2)]
where the time goes in v1:
time: 205 us
  Pallas kernels  196 us (96%)
  local copies, waits for them, and re-layouts  9.03 us (4%)
    pallas_call x1, Pallas kernels, plane_shards(): pl.pallas_call(functools.partial(plane_kernel, count, sps, pieces), out_s...  196 us

profile of v1, /device:TPU:24, one launch (start us, length us, event | category | flops | bytes accessed | tf_op | source)
XLA Modules:
  0.0 204.6 jit_solution(1836128532711008948)
XLA Ops:
  0.0 0.0 copy-start
  0.0 1.4 copy.19
  1.5 0.3 copy.20
  1.7 0.0 copy-done
  1.7 0.3 copy.21
  2.0 0.3 copy.22
  2.3 0.3 fusion
  2.6 0.0 copy-start.1
  2.7 0.0 copy-start.2
  2.7 3.3 %concatenate.3.up_own = bf16[2,256,1408]{2,1,0:T(8,128)(2,1)} concatenate(bf16[2,256,128]{2,1,0:T(8,128)(2,1)S(1)} %get-tuple-element.15, bf16[2,256,128]{2,1,0:T(8,128)(2,1)S(1)} %get-tuple-element.9, bf16[2,256,128]{2,1,0:T(8,128)(2,1)S(1)} %get-tuple-element.16, bf16[2,256,128]{2,1,0:T(8,128)(2,1)S(1)} %get-tuple-element.8, bf16[2,256,128]{2,1,0:T(8,128)(2,1)S(1)} %get-tuple-element.17, ...), dimensions={2} | concatenate | bytes 2883584 | tf_op jit(solution)/shard_map/concatenate | solution.py:1399
  6.0 0.0 copy-done.1
  6.0 0.1 reshape.30
  6.1 0.0 copy-done.2
  6.1 0.1 reshape.31
  6.2 0.6 copy_bitcast_fusion
  6.8 195.5 %plane.1 = bf16[256,2048]{1,0:T(8,128)(2,1)} custom-call(bf16[1024,256]{1,0:T(8,128)(2,1)} %q_ref.1, bf16[1024,256]{1,0:T(8,128)(2,1)} %k_ref.1, bf16[1024,512]{1,0:T(8,128)(2,1)} %v_ref.1, bf16[1024,512]{1,0:T(8,128)(2,1)} %out_gate_ref.1, f32[4,1024]{1,0:T(4,128)} %in_gate_ref.1, f32[4,1024]{1,0:T(4,128)} %forget_ref.1, f32[4,1024]{1,0:T(4,128)} %extra_ref.1, ...), custom_call_target="tpu_custom_call" | custom-call | flops 17716740096 | bytes 30000000 | tf_op jit(solution)/shard_map/plane/pallas_call | solution.py:1407
  202.3 2.3 %copy.28 = bf16[256,2048]{1,0:T(8,128)(2,1)} copy(bf16[256,2048]{1,0:T(8,128)(2,1)} %plane.1) | data formatting | bytes 2097152
  (2 shorter events, 0.0 us)
Async XLA Ops:
  0.0 1.7 copy-start
  2.6 3.3 %copy-start.1 = (bf16[3,1408]{1,0:T(4,128)(2,1)S(1)}, bf16[3,1408]{1,0:T(4,128)(2,1)}, u32[]{:S(2)}) copy-start(bf16[3,1408]{1,0:T(4,128)(2,1)} %param.33) | copy-start | bytes 25348
  2.7 3.4 %copy-start.2 = (bf16[3,1408]{1,0:T(4,128)(2,1)S(1)}, bf16[3,1408]{1,0:T(4,128)(2,1)}, u32[]{:S(2)}) copy-start(bf16[3,1408]{1,0:T(4,128)(2,1)} %param.34) | copy-start | bytes 25348

commit v2 on v1

--- a/solution.py
+++ b/solution.py
@@ -756,14 +756,16 @@
         self.y_send, self.y_recv, self.send, self.recv = y_send, y_recv, send, recv
         self.sp = lax.axis_index("sp")
         self.z, self.y = self.sp // 2, lax.rem(self.sp, 2)
-        self.units = [("up", yy, r) for yy in range(2) for r in range(2)]
-        self.units += [("down", yy, 0) for yy in range(2)]
+        self.units = [("main", yy, r) for yy in range(2) for r in range(2)]
+        self.units += [("edge", yy, 0) for yy in range(2)] + [("down", yy, 0) for yy in range(2)]
+        last = rows_z - 1
+        order = [("main", hop) for hop in range(1, last)] + [("edge", 1), ("main", last)]
+        order += [("edge", hop) for hop in range(2, last + 1)]
+        order += [("down", hop) for hop in range(1, last + 1)]
+        if last == 1:
+            order = [("main", 1), ("edge", 1), ("down", 1)]
         self.events = [
-            (unit, hop)
-            for kind in ("up", "down")
-            for hop in range(1, rows_z)
-            for unit in self.units
-            if unit[0] == kind
+            (unit, hop) for kind, hop in order for unit in self.units if unit[0] == kind
         ]
         self.waited = set()
         self.next = 0
@@ -774,8 +776,15 @@
         if kind == "down":
             return self.down_all.at[shard]
         rows = self.up_own.shape[1]
+        if kind == "edge":
+            return self.up_all.at[pl.ds(pl.multiple_of(shard * rows, rows), rows), self.cols(kind)]
         start = pl.multiple_of(shard * rows + r * (rows // 2), rows // 2)
-        return self.up_all.at[pl.ds(start, rows // 2)]
+        return self.up_all.at[pl.ds(start, rows // 2), self.cols(kind)]
+
+    def cols(self, kind):
+        width = self.up_all.shape[1]
+        main = main_tiles(width // 2) * 2 * LANES
+        return pl.ds(0, main) if kind == "main" else pl.ds(main, width - main)
 
     def own(self, unit, y):
         kind, _, r = unit
@@ -783,21 +792,23 @@
             rows = self.down_all.shape[1]
             return self.down_own.at[pl.ds(pl.multiple_of(y * rows, rows), rows)]
         rows = self.up_own.shape[1]
-        return self.up_own.at[y, pl.ds(r * (rows // 2), rows // 2)]
+        if kind == "edge":
+            return self.up_own.at[y, :, self.cols(kind)]
+        return self.up_own.at[y, pl.ds(r * (rows // 2), rows // 2), self.cols(kind)]
 
     def side(self, yy):
         return self.y if yy == 0 else 1 - self.y
 
     def across(self, unit):
-        at = self.units.index(("down" if unit[0] == "down" else "up", 1, unit[2]))
+        at = self.units.index((unit[0], 1, unit[2]))
         return remote(
             self.own(unit, 1 - self.y), self.piece(unit, self.z, self.y),
             self.y_send.at[at], self.y_recv.at[at], {"sp": self.z * 2 + 1 - self.y},
         )
 
-    def start_across(self):
+    def start_across(self, *kinds):
         for unit in self.units:
-            if unit[1] == 1:
+            if unit[1] == 1 and unit[0] in kinds:
                 self.across(unit).start()
 
     def came_across(self, unit):
@@ -854,12 +865,28 @@
             for way in range(2):
                 if hop > 1:
                     self.arrived(way, (unit, hop - 1))
-
-                @pl.when(self.sends(way, hop))
+                sends = self.sends(way, hop)
+                if unit[0] == "down" and hop == 1:
+                    sends = jnp.logical_and(sends, self.sends(way, self.rows_z - 1))
+
+                @pl.when(sends)
                 def _(way=way, event=event):
                     self.copy(way, event).start()
 
             self.next += 1
+
+    def start_down(self):
+        for event in self.events:
+            unit, hop = event
+            if unit[0] == "down" and hop == 1:
+                if unit[1] == 1:
+                    self.came_across(unit)
+                for way in range(2):
+                    last = self.sends(way, self.rows_z - 1)
+
+                    @pl.when(jnp.logical_and(self.sends(way, 1), jnp.logical_not(last)))
+                    def _(way=way, event=event):
+                        self.copy(way, event).start()
 
     def arrived_all(self, kind):
         for unit in self.units:
@@ -882,6 +909,31 @@
                     self.copy(way, event).wait_send()
 
 
+def main_tiles(hidden):
+    return max(hidden // LANES - 1, 1)
+
+
+def whole_state(heads, blocks, k_ref, v_ref, reach_ref, top_ref, state_ref, held_ref):
+    last = top_ref[:, pl.ds(blocks * CHUNK - LANES, LANES)]
+    now = jnp.broadcast_to(last[:, LANES - 1 :], last.shape)
+    held_ref[...] = now
+    state_ref[...] = jnp.zeros_like(state_ref)
+    ones = jnp.ones((CHUNK, LANES), bf16)
+    at_k = lax.broadcasted_iota(jnp.int32, (CHUNK, CHUNK), 0)
+
+    @pl.loop(0, blocks)
+    def _(b):
+        rows = pl.ds(pl.multiple_of(b * CHUNK, CHUNK), CHUNK)
+        weight = jnp.exp(reach_ref[:, rows] - now)
+        for pair in range(heads // 2):
+            turned_keys = k_ref[rows, pl.ds(pair * LANES, LANES)].astype(f32).T
+            for h in (2 * pair, 2 * pair + 1):
+                value = jnp.concatenate([v_ref[rows, pl.ds(h * VAL_DIM, VAL_DIM)], ones], axis=1)
+                own = (at_k >= KEY_DIM) if h % 2 else (at_k < KEY_DIM)
+                high, low = split(jnp.where(own, turned_keys, 0.0) * weight[h : h + 1, :])
+                state_ref[h] += mm(high, value) + mm(low, value)
+
+
 def clear_state(in_cells, in_norm, in_top, in_after):
     in_cells[...] = jnp.zeros_like(in_cells)
     in_norm[...] = jnp.zeros_like(in_norm)
@@ -897,9 +949,9 @@
     count, sps, pieces,
     q_ref, k_ref, v_ref, out_gate_ref, in_gate_ref, forget_ref, extra_ref, head_gain_ref,
     out_weight_ref, residual_ref, cell_gain_ref, ffn_gain_ref, close_gain_ref,
-    up_own, gate_taps_ref, value_taps_ref, down_own,
+    gate_up_ref, value_up_ref, gate_taps_ref, value_taps_ref, down_own,
     out_ref,
-    up_all, down_all,
+    up_own, taps_ref, up_all, down_all,
     reach_ref, top_ref, cum_ref, num_ref, den_ref, state_ref, held_ref,
     y_cells, y_small, z_cells, z_small, p_cells, p_small,
     in_cells, in_norm, in_top, in_after, enter_ref,
@@ -934,9 +986,20 @@
     friends += [{"sp": lax.rem(z + d, rows_z) * 2 + y} for d in range(1, rows_z)]
     for where in friends:
         pl.semaphore_signal(barrier, inc=1, device_id=where, device_id_type=MESH)
+    hidden = active_ref.shape[1]
+    for side in range(2):
+        for start in range(0, hidden, LANES):
+            size = min(LANES, hidden - start)
+            for at, weight in ((0, gate_up_ref), (size, value_up_ref)):
+                up_own[side, :, 2 * start + at : 2 * start + at + size] = weight[
+                    :, side * hidden + start : side * hidden + start + size
+                ]
+    for at, taps in enumerate((gate_taps_ref, value_taps_ref)):
+        both = taps[...].astype(f32)
+        taps_ref[at, 0:WIDTH, :] = jnp.where(y == 0, both[:, :hidden], both[:, hidden:])
     pl.semaphore_wait(barrier, len(friends))
 
-    line.start_across()
+    line.start_across("main")
     line.pump_to(LINE_START)
     own_rows = up_own.shape[1]
     own_up = pltpu.make_async_copy(
@@ -951,15 +1014,7 @@
     own_down.start()
 
     gate_rows_into(heads, in_gate_ref, forget_ref, extra_ref, reach_ref, top_ref, cum_ref)
-    state_ref[...] = jnp.zeros_like(state_ref)
-    held_ref[...] = jnp.full_like(held_ref, empty_log)
-
-    @pl.loop(0, blocks)
-    def _(b):
-        cell_block(
-            heads, b, q_ref, k_ref, v_ref, reach_ref, top_ref, num_ref, den_ref, state_ref, held_ref
-        )
-
+    whole_state(heads, blocks, k_ref, v_ref, reach_ref, top_ref, state_ref, held_ref)
     last = cum_ref[:, pl.ds(tok_rows - LANES, LANES)]
     cum_last = jnp.broadcast_to(last[:, LANES - 1 :], last.shape)
     pack_state(heads, state_ref, held_ref, cum_last, y_cells.at[y], y_small.at[y])
@@ -969,6 +1024,20 @@
 
     swap(y_small, y, 0).start()
     swap(y_cells, y, 1).start()
+    line.start_across("edge", "down")
+    line.pump_to(LINE_SWAP)
+    state_ref[...] = jnp.zeros_like(state_ref)
+    held_ref[...] = jnp.full_like(held_ref, empty_log)
+
+    def cell_blocks(low, high):
+        @pl.loop(low, high)
+        def _(b):
+            cell_block(
+                heads, b, q_ref, k_ref, v_ref, reach_ref, top_ref, num_ref, den_ref,
+                state_ref, held_ref,
+            )
+
+    cell_blocks(0, blocks * CELL_SPLIT // 8)
     swap(y_small, 1 - y, 0).wait_recv()
     swap(y_cells, 1 - y, 1).wait_recv()
     acc = (in_cells, in_norm, in_top, in_after)
@@ -998,7 +1067,9 @@
             for copy in along(d):
                 copy.start()
 
-    line.pump_to(LINE_STATE)
+    line.pump_to(LINE_STATE[0])
+    cell_blocks(blocks * CELL_SPLIT // 8, blocks)
+    line.pump_to(LINE_STATE[1])
     clear_state(*acc)
 
     @pl.when(y == 1)
@@ -1024,12 +1095,13 @@
             enter_ref[1, h] = low
     line.pump_to(LINE_MIX)
 
-    @pl.loop(0, blocks)
-    def _(b):
-        mix_block(
-            heads, b, q_ref, out_gate_ref, head_gain_ref, top_ref, cum_ref, num_ref, den_ref,
-            in_top, enter_ref, mixed_ref,
-        )
+    def mix_blocks(at_x):
+        @pl.loop(0, blocks // 2)
+        def _(b):
+            mix_block(
+                heads, at_x * (blocks // 2) + b, q_ref, out_gate_ref, head_gain_ref, top_ref,
+                cum_ref, num_ref, den_ref, in_top, enter_ref, mixed_ref,
+            )
 
     def product(chunk, piece, store):
         start = pl.multiple_of(chunk * rows + piece * step, step)
@@ -1043,6 +1115,7 @@
     sent, landing = [], []
     for k in (1, 0):
         to_x = x if k == 0 else 1 - x
+        mix_blocks(to_x)
         for s in range(pieces):
             span = pl.ds(s * step, step)
 
@@ -1073,7 +1146,7 @@
                 copy.start()
                 sent.append(copy)
                 landing.append(copy)
-    line.pump_to(LINE_REDUCED)
+        line.pump_to(LINE_REDUCED[1 - k])
 
     def block(side, owner, s):
         start = pl.multiple_of(HALO + side * tok_rows + owner * rows + s * step, HALO)
@@ -1137,6 +1210,7 @@
         from_d = block(1 - y, other, s)
         take(from_d, to_d, s, x_peer if s == 0 else y_peer)
         give(from_d, to_p, 3 * pieces + s, partner)
+        line.pump_to(LINE_DIAGONAL[s])
     mate, other_mate = x * CORES + 1 - core, (1 - x) * CORES + 1 - core
     for s in range(pieces):
         take(block(y, mate, s), to_p, s, partner)
@@ -1160,15 +1234,15 @@
     def _():
         normed_ref[pl.ds(0, HALO), :] = jnp.zeros((HALO, width), bf16)
 
+    line.start_down()
     line.pump_to(LINE_UP)
     own_up.wait()
-    line.arrived_all("up")
+    line.arrived_all("main")
 
     @pl.when(z > 0)
     def _():
         halo(z + rows_z - 1).wait_recv()
 
-    hidden = active_ref.shape[1]
     full, rest = hidden // LANES, hidden % LANES
 
     def up_tile(weight_cols, cols, half):
@@ -1179,22 +1253,20 @@
         @pl.loop(0, group // CONV_ROWS)
         def _(i):
             sums = []
-            for taps, side in ((gate_taps_ref, 0), (value_taps_ref, 1)):
+            for side in range(2):
                 summed = jnp.zeros((CONV_ROWS, half), f32)
                 base = pl.multiple_of(i * CONV_ROWS, CONV_ROWS)
                 window = lift_ref[pl.ds(base, CONV_ROWS + HALO), pl.ds(side * half, half)]
                 for offset in range(WIDTH):
-                    tap = taps[y, offset : offset + 1, cols].astype(f32)
+                    tap = taps_ref[side, offset : offset + 1, cols]
                     low = HALO - WIDTH + 1 + offset
                     summed = summed + tap * window[low : low + CONV_ROWS]
                 sums.append(summed)
             active = jax.nn.gelu(sums[0], approximate=True) * sums[1]
             active_ref[pl.ds(base, CONV_ROWS), cols] = active.astype(bf16)
 
-    edges = [full * i // len(LINE_TILES) for i in range(len(LINE_TILES) + 1)]
-    for i, number in enumerate(LINE_TILES):
-
-        @pl.loop(edges[i], edges[i + 1])
+    def up_tiles(low, high):
+        @pl.loop(low, high)
         def _(j):
             up_tile(
                 pl.ds(pl.multiple_of(j * 2 * LANES, 2 * LANES), 2 * LANES),
@@ -1202,9 +1274,16 @@
                 LANES,
             )
 
-        line.pump_to(number)
+    main = main_tiles(hidden)
+    up_tiles(0, main // 2)
+    line.pump_to(LINE_TILES[0])
+    up_tiles(main // 2, main)
+    line.pump_to(LINE_TILES[1])
+    line.arrived_all("edge")
+    up_tiles(main, full)
     if rest:
         up_tile(pl.ds(full * 2 * LANES, 2 * rest), pl.ds(full * LANES, rest), rest)
+    line.pump_to(LINE_TILES[2])
 
     own_down.wait()
     for copy in sent:
@@ -1213,8 +1292,6 @@
     def chunk_rows(side, at_x, at_core):
         start = side * tok_rows + (at_x * CORES + at_core) * rows
         return pl.ds(pl.multiple_of(start, rows), rows)
-
-    sides = ((1 - y, 1 - x), (y, 1 - x), (1 - y, x), (y, x))
 
     def pair_copy(shard, k):
         return remote(
@@ -1222,10 +1299,11 @@
             p2_send.at[shard, k], p2_recv.at[shard, k], partner,
         )
 
-    def one_copy(shard, at):
+    def one_copy(shard, at, where=None):
+        where = where or (x_peer if at < 2 else y_peer)
         return remote(
             one_out.at[shard, at], one_in.at[shard, at],
-            one_send.at[shard, at], one_recv.at[shard, at], x_peer if at < 2 else y_peer,
+            one_send.at[shard, at], one_recv.at[shard, at], where,
         )
 
     def two_copy(shard, at):
@@ -1234,34 +1312,44 @@
             two_send.at[shard, at], two_recv.at[shard, at], y_peer if at == 0 else x_peer,
         )
 
-    low, high = slice(0, step), slice(step, rows)
+    low, high = pl.ds(0, step), pl.ds(step, rows - step)
+
+    def side_of(k):
+        return jnp.where(lax.rem(k, 2) == 0, 1 - y, y), jnp.where(k < 2, 1 - x, x)
+
+    def part_rows(k, start, size):
+        return pl.ds(pl.multiple_of(k * rows + start, step), size)
 
     def multiply(shard):
-        weight = down_all[shard]
-        for k, (side, at_x) in enumerate(sides):
-            left = active_ref[chunk_rows(side, at_x, 1 - core), :]
-            pair_out[shard, k] = mm(left, weight).astype(bf16)
+        weight = down_all.at[shard]
+
+        @pl.loop(0, 4)
+        def _(k):
+            left = active_ref[chunk_rows(*side_of(k), 1 - core), :]
+            pair_out[shard, k] = mm(left, weight[...]).astype(bf16)
             pair_copy(shard, k).start()
-        for k, (side, at_x) in enumerate(sides):
-            left = active_ref[chunk_rows(side, at_x, core), :]
-            part = mm(left, weight).astype(bf16).astype(f32)
+
+        @pl.loop(0, 4)
+        def _(k):
+            left = active_ref[chunk_rows(*side_of(k), core), :]
+            part = mm(left, weight[...]).astype(bf16).astype(f32)
             pair_copy(shard, k).wait_recv()
-            summed = part + pair_in[shard, k].astype(f32)
-            if k == 0:
-                one_out[shard, 0] = summed[low].astype(bf16)
-                one_copy(shard, 0).start()
-                one_out[shard, 2] = summed[high].astype(bf16)
-                one_copy(shard, 2).start()
-            elif k == 1:
-                one_out[shard, 1] = summed[low].astype(bf16)
-                one_copy(shard, 1).start()
-                two_out[shard, 1] = summed[high].astype(bf16)
-            elif k == 2:
-                one_out[shard, 3] = summed[high].astype(bf16)
-                one_copy(shard, 3).start()
-                two_out[shard, 0] = summed[low].astype(bf16)
-            else:
-                total[shard] = summed
+            lift_ref[part_rows(k, 0, rows), :] = part + pair_in[shard, k].astype(f32)
+
+            @pl.when(k < 2)
+            def _():
+                one_out[shard, k] = lift_ref[part_rows(k, 0, step), :].astype(bf16)
+                one_copy(shard, k, x_peer).start()
+
+            @pl.when(lax.rem(k, 2) == 0)
+            def _():
+                at = 2 + k // 2
+                one_out[shard, at] = lift_ref[part_rows(k, step, step), :].astype(bf16)
+                one_copy(shard, at, y_peer).start()
+
+        two_out[shard, 0] = lift_ref[part_rows(2, 0, step), :].astype(bf16)
+        two_out[shard, 1] = lift_ref[part_rows(1, step, step), :].astype(bf16)
+        total[shard] = lift_ref[part_rows(3, 0, rows), :]
 
     def pass_on(shard):
         one_copy(shard, 0).wait_recv()
@@ -1291,39 +1379,37 @@
         else:
             pl.when(line.valid(way, hop))(action)
 
-    first_down = 4 * (rows_z - 1)
-    waiting = []
-    for way, hop, yy in steps:
-        unit = ("down", yy, 0)
-        if way is None:
-            if yy:
-                line.came_across(unit)
-        else:
-            line.pump_to(first_down + 2 * hop + yy + 1)
-            line.arrived(way, (unit, hop))
-        entry = (way, hop, yy)
-        shard = shard_of(way, hop, yy)
-        at_step(entry, functools.partial(multiply, shard))
-        waiting.append((entry, shard))
-        if len(waiting) > 2:
-            entry, shard = waiting.pop(0)
+    first_down = 6 * (rows_z - 1)
+    def finish(shard):
+        two_copy(shard, 0).wait_recv()
+        two_copy(shard, 1).wait_recv()
+        total[shard, low] = (
+            total[shard, low] + one_in[shard, 1].astype(f32) + two_in[shard, 0].astype(f32)
+        )
+        total[shard, high] = (
+            total[shard, high] + one_in[shard, 3].astype(f32) + two_in[shard, 1].astype(f32)
+        )
+
+    queue = []
+    for at in range(len(steps) + LAG_FINISH):
+        if at < len(steps):
+            way, hop, yy = steps[at]
+            unit = ("down", yy, 0)
+            if way is None:
+                if yy:
+                    line.came_across(unit)
+            else:
+                line.pump_to(first_down + 2 * hop + yy + 1)
+                line.arrived(way, (unit, hop))
+            queue.append((steps[at], shard_of(*steps[at])))
+            entry, shard = queue[at]
+            at_step(entry, functools.partial(multiply, shard))
+        if 0 <= at - LAG_PASS < len(steps):
+            entry, shard = queue[at - LAG_PASS]
             at_step(entry, functools.partial(pass_on, shard))
-    for entry, shard in waiting:
-        at_step(entry, functools.partial(pass_on, shard))
-    for entry in steps:
-
-        def finish(entry=entry):
-            shard = shard_of(*entry)
-            two_copy(shard, 0).wait_recv()
-            two_copy(shard, 1).wait_recv()
-            total[shard, low] = (
-                total[shard, low] + one_in[shard, 1].astype(f32) + two_in[shard, 0].astype(f32)
-            )
-            total[shard, high] = (
-                total[shard, high] + one_in[shard, 3].astype(f32) + two_in[shard, 1].astype(f32)
-            )
-
-        at_step(entry, finish)
+        if 0 <= at - LAG_FINISH < len(steps):
+            entry, shard = queue[at - LAG_FINISH]
+            at_step(entry, functools.partial(finish, shard))
     summed = total[...].astype(bf16).astype(f32)
     scale = rms_scale(total_square(summed), width)
     for j in range(sps):
@@ -1358,20 +1444,19 @@
 
 
 LINE_START = 2
-LINE_STATE = 4
-LINE_MIX = 6
-LINE_REDUCED = 9
-LINE_NORM = (10, 10)
-LINE_GATHER = (11, 12)
-LINE_UP = 14
-LINE_TILES = (14, 14)
+LINE_SWAP = 3
+LINE_STATE = (4, 6)
+LINE_MIX = 7
+LINE_REDUCED = (10, 12)
+LINE_NORM = (13, 13)
+LINE_GATHER = (14, 15)
+LINE_DIAGONAL = (16, 17)
+LINE_UP = 20
+LINE_TILES = (20, 21, 22)
+CELL_SPLIT = 4
+LAG_PASS = 4
+LAG_FINISH = 14
 CONV_ROWS = 256
-
-
-def by_side(array, axis):
-    shape = array.shape
-    parted = shape[:axis] + (2, shape[axis] // 2) + shape[axis + 1 :]
-    return jnp.moveaxis(array.reshape(parted), axis, 0)
 
 
 def plane_shards(
@@ -1391,12 +1476,6 @@
     rows = tok_rows // count
     pieces = 2
     step = rows // pieces
-    gate_parts, value_parts = by_side(gate_up_weight, 1), by_side(value_up_weight, 1)
-    tiles = []
-    for start in range(0, hidden, LANES):
-        cols = slice(start, min(start + LANES, hidden))
-        tiles += [gate_parts[:, :, cols], value_parts[:, :, cols]]
-    up_own = jnp.concatenate(tiles, axis=2)
     vmem = pl.BlockSpec(memory_space=pltpu.VMEM)
     hbm = pl.BlockSpec(memory_space=pl.ANY)
     dma = pltpu.SemaphoreType.DMA
@@ -1407,9 +1486,11 @@
     return pl.pallas_call(
         functools.partial(plane_kernel, count, sps, pieces),
         out_shape=jax.ShapeDtypeStruct(residual.shape, bf16),
-        in_specs=[vmem] * 13 + [hbm, vmem, vmem, hbm],
+        in_specs=[vmem] * 17 + [hbm],
         out_specs=vmem,
         scratch_shapes=[
+            V((2, own_depth, 2 * hidden), bf16),
+            V((2, 8, hidden), f32),
             V((own_depth * sps, 2 * hidden), bf16),
             V((sps, hidden, cw), bf16),
             V((8, tok_rows), f32),
@@ -1442,10 +1523,10 @@
             V((HALO + 2 * tok_rows, width), bf16),
             V((HALO + 2 * tok_rows, 2 * LANES), f32),
             V((2 * tok_rows, hidden), bf16),
-            dma((6,)),
-            dma((6,)),
-            dma((2, 6 * (rows_z - 1))),
-            dma((2, 6 * (rows_z - 1))),
+            dma((8,)),
+            dma((8,)),
+            dma((2, 8 * (rows_z - 1))),
+            dma((2, 8 * (rows_z - 1))),
             dma((2,)),
             dma((2,)),
             dma((2,)),
@@ -1472,8 +1553,8 @@
         queries, keys, values, output_gate_logits, log_input_gate, forget_gate_logits,
         extra_forget_terms, per_head_norm_gain.reshape(1, -1), output_weight, residual,
         after_cell_norm_gain.reshape(1, -1), feedforward_norm_gain.reshape(1, -1),
-        closing_norm_gain.reshape(1, -1), up_own, by_side(gate_filter_taps, 1),
-        by_side(value_filter_taps, 1), down_weight,
+        closing_norm_gain.reshape(1, -1), gate_up_weight, value_up_weight, gate_filter_taps,
+        value_filter_taps, down_weight,
     )
 
 
@@ -1483,8 +1564,10 @@
     plane = (
         grid_of(sps)[1] == 2
         and count == 2 * CORES
-        and own_width % LANES == 0
+        and own_width == 2 * LANES
         and hidden % 32 == 0
+        and hidden >= 4 * LANES
+        and arrays[0].shape[0] % (2 * CHUNK) == 0
     )
     return plane_shards(*arrays) if plane else ring_shards(*arrays)
 

time: 205 us -> 183 us (0.89); the launches traced: 205 us -> 180 us
  Pallas kernels: 196 us -> 178 us
  local copies, waits for them, and re-layouts: 9.03 us -> 2.3 us
    pallas_call x1, Pallas kernels: 196 us -> 178 us  [plane_shards(): pl.pallas_call(functools.partial(plane_kernel, count, sps, pieces), out_s...]
    concatenate x1 -> x0, local copies, waits for them, and re-layouts: 3.28 us -> none  [plane_shards(): up_own = jnp.concatenate(tiles, axis=2)]
where the time goes in v2:
time: 183 us; the launch traced here: 180 us
  Pallas kernels  178 us (97%)
  local copies, waits for them, and re-layouts  2.3 us (1%)
    pallas_call x1, Pallas kernels, plane_shards(): pl.pallas_call(functools.partial(plane_kernel, count, sps, pieces), out_s...  178 us

profile of v2, /device:TPU:24, one launch (start us, length us, event | category | flops | bytes accessed | tf_op | source)
XLA Modules:
  0.0 180.4 jit_solution(5955801422658763304)
XLA Ops:
  0.0 178.1 %plane.1 = bf16[256,2048]{1,0:T(8,128)(2,1)} custom-call(bf16[1024,256]{1,0:T(8,128)(2,1)} %q_ref.1, bf16[1024,256]{1,0:T(8,128)(2,1)} %k_ref.1, bf16[1024,512]{1,0:T(8,128)(2,1)} %v_ref.1, bf16[1024,512]{1,0:T(8,128)(2,1)} %out_gate_ref.1, f32[4,1024]{1,0:T(4,128)} %in_gate_ref.1, f32[4,1024]{1,0:T(4,128)} %forget_ref.1, f32[4,1024]{1,0:T(4,128)} %extra_ref.1, ...), custom_call_target="tpu_custom_call" | custom-call | flops 17716740096 | bytes 30000000 | tf_op jit(solution)/shard_map/plane/pallas_call | solution.py:1486
  178.1 2.3 %copy.20 = bf16[256,2048]{1,0:T(8,128)(2,1)} copy(bf16[256,2048]{1,0:T(8,128)(2,1)} %plane.1) | data formatting | bytes 2097152
